TPU v7x, 128 devices: a whole 4x4x4 slice. The times are simulated.
128 devices in a mesh: kv: 32 (over z, y, core), tp: 4 (over x).
Axes of the slice: x: 4, y: 4, z: 4, core: 2. Of those that a mesh axis runs over, the one named last changes fastest.
Arguments:
- queries: bfloat16 [2, 12288, 1024], P(None, 'kv', 'tp'), may hold values from -112 to 112
- key_states: bfloat16 [2, 12288, 256], P(None, 'kv', 'tp'), may hold values from -4 to 4
- value_states: bfloat16 [2, 12288, 256], P(None, 'kv', 'tp'), may hold values from -6 to 6
- cotangent: bfloat16 [2, 12288, 1024], P(None, 'kv', 'tp'), may hold values from -6 to 6
- gate_logits: float32 [2, 12288, 16], P(None, 'kv', 'tp'), may hold values from -6 to 6
- layer_input: bfloat16 [2, 12288, 4096], P(None, ('kv', 'tp')), may hold values from -6 to 6
- chosen: int32 [2, 192, 4, 16], P(None, 'kv', 'tp'), may hold values from 0 to 191, as said below
Outputs:
- query_grad: bfloat16 [2, 12288, 1024], P(None, 'kv', 'tp')
- key_grad: bfloat16 [2, 12288, 256], P(None, 'kv', 'tp')
- value_grad: bfloat16 [2, 12288, 256], P(None, 'kv', 'tp')
- value_weight_grad: float32 [4096, 256], P(('kv', 'tp'))
Inputs may be any that keep to these rules, and one draw needn't show every extreme that they name: `chosen`: for each sequence, query block b and key head, the 16 entries are distinct blocks; they include b itself and block 0; blocks after b hold only keys after all of the block's queries. Taking the 6 query blocks of one index of kv together (aligned), one sequence and one key head, at most 2 distinct blocks held by any one earlier index of kv are named, and some index reaches 2.
All inputs are finite; a program needn't handle non-finite values.
Results may differ from a plain program's by a relative error of at most 0.0058.
Values may be sent and summed in bfloat16 or wider, within the bound.
A program may use at most 128 MiB of HBM per device.

v0:
```python
import functools

import jax
import jax.numpy as jnp
from jax import lax
from jax.experimental import pallas as pl
from jax.experimental.pallas import tpu as pltpu
from jax.sharding import PartitionSpec as P

BLK = 64
MESH = pl.DeviceIdType.MESH
F32 = jnp.float32
BF16 = jnp.bfloat16
SEQS = 2
BPD = 6
ROWS = BPD * BLK
ZN = 4
YN = 4
DEVS = ZN * YN * 2
HD = 64
HEADS = 4
TOPK = 16
NEG = -1e30


def place():
    kv = lax.axis_index("kv")
    tp = lax.axis_index("tp")
    z, y, c = kv // 8, (kv // 2) % 4, kv % 2
    return kv, tp, z, y, c


def rcopy(src, dst, ssem, rsem, device):
    return pltpu.make_async_remote_copy(
        src_ref=src, dst_ref=dst, send_sem=ssem, recv_sem=rsem, device_id=device, device_id_type=MESH
    )


def entry_barrier(peers):
    sem = pltpu.get_barrier_semaphore()
    for peer in peers:
        pl.semaphore_signal(sem, inc=1, device_id=peer, device_id_type=MESH)
    pl.semaphore_wait(sem, len(peers))


def gather_kernel(k_ref, v_ref, out_ref, ssem, rsem, psend, precv):
    kv, tp, z, y, c = place()

    def zy(z_, y_):
        return (z_ % 4) * 8 + (y_ % 4) * 2 + c

    for s in range(SEQS):
        out_ref[s, kv] = jnp.concatenate([k_ref[s], v_ref[s]], axis=-1)
    partner = (kv + 1 - 2 * c, tp)
    entry_barrier([(zy(z, y + 1), tp), (zy(z, y + 3), tp), (zy(z + 1, y), tp), (zy(z + 3, y), tp), partner])

    half = ROWS // 2

    class Seq:
        def __init__(self, s):
            self.s = s
            self.base = s * 20
            self.sends = []
            self.pcount = 0

        def at(self, a, b):
            return zy(z + b, y + a) if self.s == 0 else zy(z + a, y + b)

        def dev(self, a, b):
            return (self.at(a, b), tp)

        def ref(self, a, b, part):
            chunk = out_ref.at[self.s, self.at(a, b)]
            if part is None:
                return chunk
            return chunk.at[pl.ds(part * half, half)]

        def send(self, i, a, b, part, to):
            r = self.ref(a, b, part)
            d = rcopy(r, r, ssem.at[self.base + i], rsem.at[self.base + i], self.dev(*to))
            d.start()
            self.sends.append(d)

        def recv(self, i, a, b, part):
            r = self.ref(a, b, part)
            rcopy(r, r, ssem.at[self.base + i], rsem.at[self.base + i], self.dev(0, 0)).wait_recv()

        def share(self, a, b):
            i = self.s * 16 + self.pcount
            self.pcount += 1
            r = self.ref(a, b, None)
            d = rcopy(r, r, psend.at[i], precv.at[i], partner)
            d.start()
            self.sends.append(d)

        def first(self):
            self.send(0, 0, 0, None, (1, 0))
            self.send(1, 0, 0, None, (-1, 0))
            self.second_start(0, 0)
            self.share(0, 0)

        def second_start(self, q, a):
            self.send(4 + 4 * q, a, 0, None, (0, 1))
            self.send(5 + 4 * q, a, 0, None, (0, -1))

        def second_forward(self, q, a):
            self.recv(4 + 4 * q, a, -1, None)
            self.send(6 + 4 * q, a, -1, 0, (0, 1))
            self.recv(5 + 4 * q, a, 1, None)
            self.send(7 + 4 * q, a, 1, 1, (0, -1))
            self.share(a, -1)
            self.share(a, 1)

        def second_end(self, q, a):
            self.recv(6 + 4 * q, a, 2, 0)
            self.recv(7 + 4 * q, a, 2, 1)
            self.share(a, 2)

        def first_forward(self):
            self.recv(0, -1, 0, None)
            self.send(2, -1, 0, 0, (1, 0))
            self.recv(1, 1, 0, None)
            self.send(3, 1, 0, 1, (-1, 0))
            self.second_start(1, -1)
            self.second_start(2, 1)
            self.share(-1, 0)
            self.share(1, 0)

        def first_end(self):
            self.recv(2, 2, 0, 0)
            self.recv(3, 2, 0, 1)
            self.second_start(3, 2)
            self.share(2, 0)

    seqs = [Seq(0), Seq(1)]
    for q in seqs:
        q.first()
    for q in seqs:
        q.first_forward()
    for q in seqs:
        q.second_forward(0, 0)
    for q in seqs:
        q.first_end()
    for q in seqs:
        q.second_forward(1, -1)
    for q in seqs:
        q.second_end(0, 0)
    for q in seqs:
        q.second_forward(2, 1)
    for q in seqs:
        q.second_end(1, -1)
    for q in seqs:
        q.second_forward(3, 2)
    for q in seqs:
        q.second_end(2, 1)
    for q in seqs:
        q.second_end(3, 2)
    order = [(0, 0), (-1, 0), (1, 0), (0, -1), (0, 1), (2, 0), (-1, -1), (-1, 1), (0, 2), (1, -1), (1, 1),
             (-1, 2), (2, -1), (2, 1), (1, 2), (2, 2)]
    for s in range(SEQS):
        q = seqs[s]
        for n, (a, b) in enumerate(order):
            r = out_ref.at[s, q.at(a, b) + 1 - 2 * c]
            rcopy(r, r, psend.at[s * 16 + n], precv.at[s * 16 + n], partner).wait_recv()
    for q in seqs:
        for d in q.sends:
            d.wait_send()


def gather_kv(keys, values):
    return pl.pallas_call(
        gather_kernel,
        out_shape=jax.ShapeDtypeStruct((SEQS, DEVS, ROWS, 2 * HD), BF16),
        in_specs=[pl.BlockSpec(memory_space=pltpu.VMEM)] * 2,
        out_specs=pl.BlockSpec(memory_space=pltpu.VMEM),
        scratch_shapes=[
            pltpu.SemaphoreType.DMA((40,)),
            pltpu.SemaphoreType.DMA((40,)),
            pltpu.SemaphoreType.DMA((32,)),
            pltpu.SemaphoreType.DMA((32,)),
        ],
        compiler_params=pltpu.CompilerParams(
            collective_id=0, has_side_effects=True, vmem_limit_bytes=16 * 2**20
        ),
        name="gather_kv",
    )(keys, values)


def attend_kernel(
    ids_ref, kv_ref, q_ref, g_ref, gate_ref, dq_ref, table_ref, acc, kvbuf, rows_buf, scores, packed
):
    s = pl.program_id(0)
    qb = pl.program_id(1)
    keys = TOPK * BLK
    nrow = HEADS * BLK

    @pl.when(qb == 0)
    def _():
        def clear(i, carry):
            acc[pl.ds(i * 6, 6)] = jnp.zeros((6, BLK, 2 * HD), F32)
            return carry

        lax.fori_loop(0, DEVS, clear, 0)

    block = lax.axis_index("kv") * BPD + qb
    base = (s * BPD + qb) * TOPK
    picked = [ids_ref[base + k] for k in range(TOPK)]
    for k in range(TOPK):
        kvbuf[k * BLK : (k + 1) * BLK] = kv_ref[0, picked[k]]

    lane = lax.broadcasted_iota(jnp.int32, (BLK, 2 * HD), 1)
    low = lane < HD
    for h in range(HEADS):
        pair = slice((h // 2) * 128, (h // 2) * 128 + 128)
        qv = q_ref[0, :, pair].astype(F32) * 0.125
        gate = jax.nn.sigmoid(gate_ref[0, :, h : h + 1])
        gv = gate * g_ref[0, :, pair].astype(F32)
        if h % 2 == 0:
            gv = pltpu.roll(gv, HD, 1)
        else:
            qv = pltpu.roll(qv, HD, 1)
        rows_buf[h * BLK : (h + 1) * BLK] = jnp.where(low, qv, 0.0).astype(BF16)
        rows_buf[nrow + h * BLK : nrow + (h + 1) * BLK] = jnp.where(low, 0.0, gv).astype(BF16)

    scores[...] = lax.dot_general(
        kvbuf[...], rows_buf[...], (((1,), (1,)), ((), ())), preferred_element_type=F32
    )
    qpos = block * BLK + lax.broadcasted_iota(jnp.int32, (BLK, nrow), 1) % BLK
    koff = lax.broadcasted_iota(jnp.int32, (BLK, nrow), 0)
    ahead = koff - qpos

    def masked(k):
        sc = scores[k * BLK : (k + 1) * BLK, :nrow]
        return jnp.where(ahead <= -(picked[k] * BLK), sc, NEG)

    top = None
    for k in range(TOPK):
        m = masked(k).reshape(8, 8, nrow)
        m = jnp.max(m, axis=0)
        top = m if top is None else jnp.maximum(top, m)
    top = jnp.max(top, axis=0, keepdims=True)
    total = jnp.zeros((8, nrow), F32)
    for k in range(TOPK):
        e = jnp.exp(masked(k) - top)
        scores[k * BLK : (k + 1) * BLK, :nrow] = e
        total = total + jnp.sum(e.reshape(8, 8, nrow), axis=0)
    inv = 1.0 / jnp.sum(total, axis=0, keepdims=True)
    dot = jnp.zeros((8, nrow), F32)
    for k in range(TOPK):
        rows = slice(k * BLK, (k + 1) * BLK)
        w = (scores[rows, :nrow] * inv).astype(BF16)
        packed[rows, nrow:] = w
        t = w.astype(F32) * scores[rows, nrow:]
        dot = dot + jnp.sum(t.reshape(8, 8, nrow), axis=0)
    row_dot = jnp.sum(dot, axis=0, keepdims=True)
    for k in range(TOPK):
        rows = slice(k * BLK, (k + 1) * BLK)
        ds = (scores[rows, :nrow] * inv) * (scores[rows, nrow:] - row_dot)
        packed[rows, :nrow] = ds.astype(BF16)

    pick = jnp.dot(packed[...], rows_buf[...], preferred_element_type=F32)
    for k in range(TOPK):
        acc[picked[k]] += pick[k * BLK : (k + 1) * BLK]
    dq_t = jnp.dot(kvbuf[...].T, packed[:, :nrow], preferred_element_type=F32)
    dq = (dq_t[:HD] * 0.125).T
    dq_ref[0] = jnp.concatenate([dq[h * BLK : (h + 1) * BLK] for h in range(HEADS)], axis=1).astype(BF16)

    @pl.when(qb == BPD - 1)
    def _():
        def put(i, carry):
            table_ref[0, pl.ds(i * 6, 6)] = acc[pl.ds(i * 6, 6)].astype(BF16)
            return carry

        lax.fori_loop(0, DEVS, put, 0)


def attend(ids, kv_all, queries, cotangent, gates):
    nblk = DEVS * BPD
    keys = TOPK * BLK
    nrow = HEADS * BLK
    return pl.pallas_call(
        attend_kernel,
        grid_spec=pltpu.PrefetchScalarGridSpec(
            num_scalar_prefetch=1,
            grid=(SEQS, BPD),
            in_specs=[
                pl.BlockSpec((1, nblk, BLK, 2 * HD), lambda s, q, ids: (s, 0, 0, 0)),
                pl.BlockSpec((1, BLK, HEADS * HD), lambda s, q, ids: (s, q, 0)),
                pl.BlockSpec((1, BLK, HEADS * HD), lambda s, q, ids: (s, q, 0)),
                pl.BlockSpec((1, BLK, HEADS), lambda s, q, ids: (s, q, 0)),
            ],
            out_specs=[
                pl.BlockSpec((1, BLK, HEADS * HD), lambda s, q, ids: (s, q, 0)),
                pl.BlockSpec((1, nblk, BLK, 2 * HD), lambda s, q, ids: (s, 0, 0, 0)),
            ],
            scratch_shapes=[
                pltpu.VMEM((nblk, BLK, 2 * HD), F32),
                pltpu.VMEM((keys, 2 * HD), BF16),
                pltpu.VMEM((2 * nrow, 2 * HD), BF16),
                pltpu.VMEM((keys, 2 * nrow), F32),
                pltpu.VMEM((keys, 2 * nrow), BF16),
            ],
        ),
        out_shape=[
            jax.ShapeDtypeStruct((SEQS, ROWS, HEADS * HD), BF16),
            jax.ShapeDtypeStruct((SEQS, nblk, BLK, 2 * HD), BF16),
        ],
        compiler_params=pltpu.CompilerParams(
            vmem_limit_bytes=44 * 2**20, dimension_semantics=("arbitrary", "arbitrary")
        ),
        name="attend",
    )(ids, kv_all.reshape(SEQS, nblk, BLK, 2 * HD), queries, cotangent, gates)


class Ring:
    def __init__(self, pos, plus, minus, bufs, ssem, rsem):
        self.pos, self.plus, self.minus = pos, plus, minus
        self.sb, self.rb = bufs
        self.ssem, self.rsem = ssem, rsem
        self.sends = []

    def copy(self, i, dev):
        return rcopy(self.sb.at[i], self.rb.at[i], self.ssem.at[i], self.rsem.at[i], dev)

    def send(self, i, dev, value):
        self.sb[i] = value.astype(BF16)
        d = self.copy(i, dev)
        d.start()
        self.sends.append(d)

    def got(self, i):
        self.copy(i, self.plus).wait_recv()
        return self.rb[i].astype(F32)

    def start(self, part):
        p = self.pos
        self.send(0, self.plus, part((p + 2) % 4, 0))
        self.send(1, self.minus, part((p + 2) % 4, 1))

    def near(self, part):
        p = self.pos
        self.send(3, self.plus, part((p + 1) % 4, 1))
        self.send(4, self.minus, part((p + 3) % 4, 0))

    def middle(self, part):
        p = self.pos
        self.send(2, self.plus, part((p + 1) % 4, 0) + self.got(0))
        self.send(5, self.minus, part((p + 3) % 4, 1) + self.got(1))

    def end(self, part):
        p = self.pos
        first = part(p, 0) + self.got(2) + self.got(4)
        second = part(p, 1) + self.got(3) + self.got(5)
        return first, second

    def drain(self):
        for d in self.sends:
            d.wait_send()


def reduce_kernel(
    table, x_in, kg_ref, vg_ref, wg_ref,
    mate, acc, sa0, ra0, sa1, ra1, sb0, rb0, sb1, rb1,
    vsend, vland, li_t, rhs, part_w, mate_w, acc_x, acc_y, sx, rx, sy, ry, sz, rz,
    s_mate, r_mate, s_ring, r_ring, s_x, r_x, s_w, r_w,
):
    kv, tp, z, y, c = place()

    def zy(z_, y_):
        return ((z_ % 4) * 8 + (y_ % 4) * 2 + c, tp)

    partner = (kv + 1 - 2 * c, tp)
    xs = [(kv, (tp + d) % 4) for d in (1, 2, 3)]
    yp, ym, zp, zm = zy(z, y + 1), zy(z, y + 3), zy(z + 1, y), zy(z + 3, y)
    entry_barrier([partner, yp, ym, zp, zm] + xs)
    other = 1 - c
    sends = []

    for g in (2, 1, 3, 0):
        for s in range(SEQS):
            if s == 0:
                src = table.at[s, :, (y + g) % 4, other]
                dst = mate.at[s, :, (y + g) % 4]
            else:
                src = table.at[s, (z + g) % 4, :, other]
                dst = mate.at[s, (z + g) % 4]
            d = rcopy(src, dst, s_mate.at[s * 4 + g], r_mate.at[s * 4 + g], partner)
            d.start()
            sends.append(d)

    def mate_ready(s, g):
        dst = mate.at[s, :, (y + g) % 4] if s == 0 else mate.at[s, (z + g) % 4]
        rcopy(dst, dst, s_mate.at[s * 4 + g], r_mate.at[s * 4 + g], partner).wait_recv()

    def first_part(s):
        def part(d, h):
            if s == 0:
                a, b = table[s, 2 * h : 2 * h + 2, d, c], mate[s, 2 * h : 2 * h + 2, d]
            else:
                a, b = table[s, d, 2 * h : 2 * h + 2, c], mate[s, d, 2 * h : 2 * h + 2]
            return a.astype(F32) + b.astype(F32)

        return part

    rings_a = [
        Ring(y, yp, ym, (sa0, ra0), s_ring.at[0], r_ring.at[0]),
        Ring(z, zp, zm, (sa1, ra1), s_ring.at[1], r_ring.at[1]),
    ]
    rings_b = [
        Ring(z, zp, zm, (sb0, rb0), s_ring.at[2], r_ring.at[2]),
        Ring(y, yp, ym, (sb1, rb1), s_ring.at[3], r_ring.at[3]),
    ]
    for s in range(SEQS):
        mate_ready(s, 2)
        rings_a[s].start(first_part(s))
    for s in range(SEQS):
        mate_ready(s, 1)
        mate_ready(s, 3)
        rings_a[s].near(first_part(s))
    for s in range(SEQS):
        rings_a[s].middle(first_part(s))

    def turn(i, carry):
        lo = pl.multiple_of(i * 512, 512)
        for s in range(SEQS):
            li_t[pl.ds(lo, 512), s * 96 : (s + 1) * 96] = x_in[s, :, pl.ds(lo, 512)].T
        return carry

    lax.fori_loop(0, 8, turn, 0)

    half = ROWS // 2

    def second_part(s):
        def part(d, h):
            return acc[s, d, h * half : (h + 1) * half]

        return part

    for s in range(SEQS):
        mate_ready(s, 0)
        first, second = rings_a[s].end(first_part(s))
        acc[s, 0:2] = first
        acc[s, 2:4] = second
        rings_b[s].start(second_part(s))
        rings_b[s].near(second_part(s))
    for s in range(SEQS):
        rings_b[s].middle(second_part(s))
    for s in range(SEQS):
        first, second = rings_b[s].end(second_part(s))
        for h, value in enumerate((first, second)):
            rows = slice(h * half, (h + 1) * half)
            value = value.astype(BF16)
            vsend[s, rows] = value
            kg_ref[s, rows] = value[:, :HD]
            vg_ref[s, rows] = value[:, HD:]

    quarter = ROWS // 4
    for n in range(3):
        to = (tp + n + 1) % 4
        lo = pl.multiple_of(to * quarter, quarter)
        d = rcopy(vsend.at[:, pl.ds(lo, quarter)], vland.at[tp], s_x.at[n], r_x.at[n], (kv, to))
        d.start()
        sends.append(d)
    vland[tp] = vsend[:, pl.ds(pl.multiple_of(tp * quarter, quarter), quarter)]
    for n in range(3):
        frm = (tp + 3 - n) % 4
        d = rcopy(vland.at[frm], vland.at[frm], s_x.at[n], r_x.at[n], (kv, frm))
        d.wait_recv()
    lane = lax.broadcasted_iota(jnp.int32, (quarter, 2 * HD), 1)
    for s in range(SEQS):
        for p in range(2):
            even = pltpu.roll(vland[2 * p, s].astype(F32), HD, 1)
            odd = vland[2 * p + 1, s].astype(F32)
            rhs[s * quarter : (s + 1) * quarter, p * 128 : (p + 1) * 128] = jnp.where(
                lane < HD, even, odd
            ).astype(BF16)

    def product(i, carry):
        lo = pl.multiple_of(i * 256, 256)
        w = jnp.dot(li_t[pl.ds(lo, 256)], rhs[...], preferred_element_type=F32)
        part_w[i] = w.reshape(2, 4, 32, 256).astype(BF16)
        return carry

    lax.fori_loop(0, 16, product, 0)
    d = rcopy(part_w.at[:, other], mate_w, s_w.at[0, 0], r_w.at[0, 0], partner)
    d.start()
    sends.append(d)
    d.wait_recv()

    def w_part(d, h):
        a = part_w[8 * h : 8 * h + 8, c, d]
        return a.astype(F32) + mate_w[8 * h : 8 * h + 8, d].astype(F32)

    ring_x = Ring(tp, xs[0], xs[2], (sx, rx), s_w.at[1], r_w.at[1])
    ring_x.start(w_part)
    ring_x.near(w_part)
    ring_x.middle(w_part)
    first, second = ring_x.end(w_part)
    acc_x[0:2] = first.reshape(2, 4, 32, 256)
    acc_x[2:4] = second.reshape(2, 4, 32, 256)

    def y_part(d, h):
        return acc_x[2 * h : 2 * h + 2, d]

    ring_y = Ring(y, yp, ym, (sy, ry), s_w.at[2], r_w.at[2])
    ring_y.start(y_part)
    ring_y.near(y_part)
    ring_y.middle(y_part)
    first, second = ring_y.end(y_part)
    acc_y[0:2] = first
    acc_y[2:4] = second

    def z_part(d, h):
        return acc_y[d, 16 * h : 16 * h + 16]

    ring_z = Ring(z, zp, zm, (sz, rz), s_w.at[3], r_w.at[3])
    ring_z.start(z_part)
    ring_z.near(z_part)
    ring_z.middle(z_part)
    first, second = ring_z.end(z_part)
    wg_ref[0:16] = first
    wg_ref[16:32] = second

    for d in sends:
        d.wait_send()
    for r in rings_a + rings_b + [ring_x, ring_y, ring_z]:
        r.drain()


def reduce_grads(table, layer_input):
    v = pltpu.VMEM
    return pl.pallas_call(
        reduce_kernel,
        out_shape=[
            jax.ShapeDtypeStruct((SEQS, ROWS, HD), BF16),
            jax.ShapeDtypeStruct((SEQS, ROWS, HD), BF16),
            jax.ShapeDtypeStruct((32, 256), F32),
        ],
        in_specs=[pl.BlockSpec(memory_space=v)] * 2,
        out_specs=[pl.BlockSpec(memory_space=v)] * 3,
        scratch_shapes=[
            v((SEQS, ZN, YN, ROWS, 2 * HD), BF16),
            v((SEQS, 4, ROWS, 2 * HD), F32),
            *[v((6, 2, ROWS, 2 * HD), BF16) for _ in range(4)],
            *[v((6, ROWS // 2, 2 * HD), BF16) for _ in range(4)],
            v((SEQS, ROWS, 2 * HD), BF16),
            v((4, SEQS, ROWS // 4, 2 * HD), BF16),
            v((4096, 192), BF16),
            v((192, 256), BF16),
            v((16, 2, 4, 32, 256), BF16),
            v((16, 4, 32, 256), BF16),
            v((4, 4, 32, 256), F32),
            v((4, 32, 256), F32),
            *[v((6, 8, 32, 256), BF16) for _ in range(2)],
            *[v((6, 2, 32, 256), BF16) for _ in range(2)],
            *[v((6, 16, 256), BF16) for _ in range(2)],
            pltpu.SemaphoreType.DMA((8,)),
            pltpu.SemaphoreType.DMA((8,)),
            pltpu.SemaphoreType.DMA((4, 6)),
            pltpu.SemaphoreType.DMA((4, 6)),
            pltpu.SemaphoreType.DMA((3,)),
            pltpu.SemaphoreType.DMA((3,)),
            pltpu.SemaphoreType.DMA((4, 6)),
            pltpu.SemaphoreType.DMA((4, 6)),
        ],
        compiler_params=pltpu.CompilerParams(
            collective_id=1, has_side_effects=True, vmem_limit_bytes=44 * 2**20
        ),
        name="reduce_grads",
    )(table.reshape(SEQS, ZN, YN, 2, ROWS, 2 * HD), layer_input)


def on_device(queries, key_states, value_states, cotangent, gate_logits, layer_input, chosen):
    kv_all = gather_kv(key_states, value_states)
    query_grad, table = attend(chosen.reshape(-1), kv_all, queries, cotangent, gate_logits)
    key_grad, value_grad, weight_grad = reduce_grads(table, layer_input)
    return query_grad, key_grad, value_grad, weight_grad


def solution(mesh):
    placed = (
        P(None, "kv", "tp"),
        P(None, "kv", "tp"),
        P(None, "kv", "tp"),
        P(None, "kv", "tp"),
        P(None, "kv", "tp"),
        P(None, ("kv", "tp"), None),
        P(None, "kv", "tp", None),
    )
    return jax.shard_map(
        on_device,
        mesh=mesh,
        in_specs=placed,
        out_specs=(P(None, "kv", "tp"), P(None, "kv", "tp"), P(None, "kv", "tp"), P(("kv", "tp"), None)),
        check_vma=False,
    )
```

profile of v0, /device:TPU:0, one launch (start us, length us, event | category | flops | bytes accessed | tf_op | source)
XLA Modules:
  0.0 120.8 jit_solution(11635466335126977945)
XLA Ops:
  0.6 0.0 copy-start.3
  0.6 0.0 copy-start.2
  0.7 0.8 reduce
  1.4 0.1 reshape.17.ids_ref
  1.5 1.1 copy.11.k_ref
  2.6 1.1 copy.12.v_ref
  3.6 0.9 copy.13.gate_ref
  4.5 0.0 copy-start.1
  4.6 29.8 %gather_kv.1 = bf16[2,32,384,128]{3,2,1,0:T(8,128)(2,1)S(1)} custom-call(bf16[2,384,64]{2,1,0:T(8,128)(2,1)S(1)} %copy.11.k_ref, bf16[2,384,64]{2,1,0:T(8,128)(2,1)S(1)} %copy.12.v_ref), custom_call_target="tpu_custom_call" | custom-call | tf_op jit(solution)/shard_map/gather_kv/pallas_call | solution.py:171
  34.4 0.0 copy-start
  34.4 2.6 %copy-done = bf16[2,32,384,128]{3,2,1,0:T(8,128)(2,1)} copy-done((bf16[2,32,384,128]{3,2,1,0:T(8,128)(2,1)}, bf16[2,32,384,128]{3,2,1,0:T(8,128)(2,1)S(1)}, u32[]{:S(2)}) %copy-start) | copy-done | bytes 6291480
  37.0 0.0 copy-done.3
  37.0 0.0 copy-done.2
  37.0 24.2 %attend.1 = (bf16[2,384,256]{2,1,0:T(8,128)(2,1)}, bf16[2,192,64,128]{3,2,1,0:T(8,128)(2,1)S(1)}) custom-call(s32[192]{0:T(256)S(1)} %reshape.17.ids_ref, bf16[2,192,64,128]{3,2,1,0:T(8,128)(2,1)} %bitcast.2, bf16[2,384,256]{2,1,0:T(8,128)(2,1)S(1)} %copy-done.2, bf16[2,384,256]{2,1,0:T(8,128)(2,1)S(1)} %copy-done.3, f32[2,384,4]{2,1,0:T(8,128)S(1)} %copy.13.gate_ref), custom_call_target="tpu_custom_call" | custom-call | tf_op jit(solution)/shard_map/attend/pallas_call | solution.py:281
  61.2 0.0 copy-done.1
  61.2 57.4 %reduce_grads.1 = (bf16[2,384,64]{2,1,0:T(8,128)(2,1)S(1)}, bf16[2,384,64]{2,1,0:T(8,128)(2,1)S(1)}, f32[32,256]{1,0:T(8,128)S(1)}) custom-call(bf16[2,4,4,2,384,128]{5,4,3,2,1,0:T(8,128)(2,1)S(1)} %bitcast.3, bf16[2,96,4096]{2,1,0:T(8,128)(2,1)S(1)} %copy-done.1), custom_call_target="tpu_custom_call" | custom-call | tf_op jit(solution)/shard_map/reduce_grads/pallas_call | solution.py:532
  118.6 0.8 copy.14
  119.4 0.8 copy.15
  120.2 0.6 copy.17
Async XLA Ops:
  0.6 36.4 %copy-start.3 = (bf16[2,384,256]{2,1,0:T(8,128)(2,1)S(1)}, bf16[2,384,256]{2,1,0:T(8,128)(2,1)}, u32[]{:S(2)}) copy-start(bf16[2,384,256]{2,1,0:T(8,128)(2,1)} %g_ref.1) | copy-start | bytes 1179652
  0.6 36.4 %copy-start.2 = (bf16[2,384,256]{2,1,0:T(8,128)(2,1)S(1)}, bf16[2,384,256]{2,1,0:T(8,128)(2,1)}, u32[]{:S(2)}) copy-start(bf16[2,384,256]{2,1,0:T(8,128)(2,1)} %q_ref.1) | copy-start | bytes 1179652
  4.5 56.7 %copy-start.1 = (bf16[2,96,4096]{2,1,0:T(8,128)(2,1)S(1)}, bf16[2,96,4096]{2,1,0:T(8,128)(2,1)}, u32[]{:S(2)}) copy-start(bf16[2,96,4096]{2,1,0:T(8,128)(2,1)} %x_in.1) | copy-start | bytes 4718596
  34.4 2.6 %copy-start = (bf16[2,32,384,128]{3,2,1,0:T(8,128)(2,1)}, bf16[2,32,384,128]{3,2,1,0:T(8,128)(2,1)S(1)}, u32[]{:S(2)}) copy-start(bf16[2,32,384,128]{3,2,1,0:T(8,128)(2,1)S(1)} %gather_kv.1) | copy-start | bytes 18874372
where the time goes:
time: 122 us; the launch traced here: 121 us
  Pallas kernels  111 us (91%)
  local copies, waits for them, and re-layouts  7.89 us (6%)
    pallas_call x1, Pallas kernels, reduce_grads(): pl.pallas_call(reduce_kernel, out_shape=[jax.ShapeDtypeStruct((SEQS, ROWS...  57.4 us
    pallas_call x1, Pallas kernels, gather_kv(): pl.pallas_call(gather_kernel, out_shape=jax.ShapeDtypeStruct((SEQS, DEVS,...  29.8 us
    pallas_call x1, Pallas kernels, attend(): pl.pallas_call(attend_kernel, grid_spec=pltpu.PrefetchScalarGridSpec(num_...  24.2 us
    unnamed x14, local copies, waits for them, and re-layouts  7.81 us

commit v1 on v0

--- a/solution.py
+++ b/solution.py
@@ -50,7 +50,7 @@
         return (z_ % 4) * 8 + (y_ % 4) * 2 + c
 
     for s in range(SEQS):
-        out_ref[s, kv] = jnp.concatenate([k_ref[s], v_ref[s]], axis=-1)
+        out_ref[s, kv] = jnp.concatenate([k_ref[s], v_ref[s]], axis=0).T
     partner = (kv + 1 - 2 * c, tp)
     entry_barrier([(zy(z, y + 1), tp), (zy(z, y + 3), tp), (zy(z + 1, y), tp), (zy(z + 3, y), tp), partner])
 
@@ -96,6 +96,8 @@
         def first(self):
             self.send(0, 0, 0, None, (1, 0))
             self.send(1, 0, 0, None, (-1, 0))
+
+        def own(self):
             self.second_start(0, 0)
             self.share(0, 0)
 
@@ -135,6 +137,8 @@
     seqs = [Seq(0), Seq(1)]
     for q in seqs:
         q.first()
+    for q in seqs:
+        q.own()
     for q in seqs:
         q.first_forward()
     for q in seqs:
@@ -187,7 +191,7 @@
 
 
 def attend_kernel(
-    ids_ref, kv_ref, q_ref, g_ref, gate_ref, dq_ref, table_ref, acc, kvbuf, rows_buf, scores, packed
+    ids_ref, kv_ref, q_ref, g_ref, gate_ref, dq_ref, table_ref, acc, kvbuf, rows_buf, scores, packed, gates_t
 ):
     s = pl.program_id(0)
     qb = pl.program_id(1)
@@ -201,19 +205,20 @@
             return carry
 
         lax.fori_loop(0, DEVS, clear, 0)
+        gates_t[...] = jax.nn.sigmoid(gate_ref[s]).T
 
     block = lax.axis_index("kv") * BPD + qb
-    base = (s * BPD + qb) * TOPK
-    picked = [ids_ref[base + k] for k in range(TOPK)]
+    picked = [ids_ref[s, qb, 0, k] for k in range(TOPK)]
     for k in range(TOPK):
-        kvbuf[k * BLK : (k + 1) * BLK] = kv_ref[0, picked[k]]
+        kvbuf[k * BLK : (k + 1) * BLK] = kv_ref[s, picked[k]]
 
     lane = lax.broadcasted_iota(jnp.int32, (BLK, 2 * HD), 1)
     low = lane < HD
+    gates = gates_t[pl.ds(pl.multiple_of(qb * BLK, BLK), BLK)]
     for h in range(HEADS):
         pair = slice((h // 2) * 128, (h // 2) * 128 + 128)
         qv = q_ref[0, :, pair].astype(F32) * 0.125
-        gate = jax.nn.sigmoid(gate_ref[0, :, h : h + 1])
+        gate = gates[:, h : h + 1]
         gv = gate * g_ref[0, :, pair].astype(F32)
         if h % 2 == 0:
             gv = pltpu.roll(gv, HD, 1)
@@ -268,7 +273,7 @@
     @pl.when(qb == BPD - 1)
     def _():
         def put(i, carry):
-            table_ref[0, pl.ds(i * 6, 6)] = acc[pl.ds(i * 6, 6)].astype(BF16)
+            table_ref[s, pl.ds(i * 6, 6)] = acc[pl.ds(i * 6, 6)].astype(BF16)
             return carry
 
         lax.fori_loop(0, DEVS, put, 0)
@@ -284,14 +289,14 @@
             num_scalar_prefetch=1,
             grid=(SEQS, BPD),
             in_specs=[
-                pl.BlockSpec((1, nblk, BLK, 2 * HD), lambda s, q, ids: (s, 0, 0, 0)),
+                pl.BlockSpec(memory_space=pltpu.VMEM),
                 pl.BlockSpec((1, BLK, HEADS * HD), lambda s, q, ids: (s, q, 0)),
                 pl.BlockSpec((1, BLK, HEADS * HD), lambda s, q, ids: (s, q, 0)),
-                pl.BlockSpec((1, BLK, HEADS), lambda s, q, ids: (s, q, 0)),
+                pl.BlockSpec(memory_space=pltpu.VMEM),
             ],
             out_specs=[
                 pl.BlockSpec((1, BLK, HEADS * HD), lambda s, q, ids: (s, q, 0)),
-                pl.BlockSpec((1, nblk, BLK, 2 * HD), lambda s, q, ids: (s, 0, 0, 0)),
+                pl.BlockSpec(memory_space=pltpu.VMEM),
             ],
             scratch_shapes=[
                 pltpu.VMEM((nblk, BLK, 2 * HD), F32),
@@ -299,6 +304,7 @@
                 pltpu.VMEM((2 * nrow, 2 * HD), BF16),
                 pltpu.VMEM((keys, 2 * nrow), F32),
                 pltpu.VMEM((keys, 2 * nrow), BF16),
+                pltpu.VMEM((ROWS, HEADS), F32),
             ],
         ),
         out_shape=[
@@ -306,7 +312,7 @@
             jax.ShapeDtypeStruct((SEQS, nblk, BLK, 2 * HD), BF16),
         ],
         compiler_params=pltpu.CompilerParams(
-            vmem_limit_bytes=44 * 2**20, dimension_semantics=("arbitrary", "arbitrary")
+            vmem_limit_bytes=24 * 2**20, dimension_semantics=("arbitrary", "arbitrary")
         ),
         name="attend",
     )(ids, kv_all.reshape(SEQS, nblk, BLK, 2 * HD), queries, cotangent, gates)
@@ -361,8 +367,8 @@
 def reduce_kernel(
     table, x_in, kg_ref, vg_ref, wg_ref,
     mate, acc, sa0, ra0, sa1, ra1, sb0, rb0, sb1, rb1,
-    vsend, vland, li_t, rhs, part_w, mate_w, acc_x, acc_y, sx, rx, sy, ry, sz, rz,
-    s_mate, r_mate, s_ring, r_ring, s_x, r_x, s_w, r_w,
+    vsend, vland, li_t, rhs, part_w, mate_w, acc_x, wsend, wland, sx, rx,
+    s_mate, r_mate, s_ring, r_ring, s_x, r_x, s_w, r_w, s_d, r_d,
 ):
     kv, tp, z, y, c = place()
 
@@ -372,7 +378,8 @@
     partner = (kv + 1 - 2 * c, tp)
     xs = [(kv, (tp + d) % 4) for d in (1, 2, 3)]
     yp, ym, zp, zm = zy(z, y + 1), zy(z, y + 3), zy(z + 1, y), zy(z + 3, y)
-    entry_barrier([partner, yp, ym, zp, zm] + xs)
+    offsets = [(dz, dy) for dz in (2, 1, 3, 0) for dy in (2, 1, 3, 0)][:-1]
+    entry_barrier([partner] + xs + [zy(z + dz, y + dy) for dz, dy in offsets])
     other = 1 - c
     sends = []
 
@@ -451,8 +458,6 @@
             rows = slice(h * half, (h + 1) * half)
             value = value.astype(BF16)
             vsend[s, rows] = value
-            kg_ref[s, rows] = value[:, :HD]
-            vg_ref[s, rows] = value[:, HD:]
 
     quarter = ROWS // 4
     for n in range(3):
@@ -461,6 +466,10 @@
         d = rcopy(vsend.at[:, pl.ds(lo, quarter)], vland.at[tp], s_x.at[n], r_x.at[n], (kv, to))
         d.start()
         sends.append(d)
+    for s in range(SEQS):
+        turned = vsend[s].T
+        kg_ref[s] = turned[:HD]
+        vg_ref[s] = turned[HD:]
     vland[tp] = vsend[:, pl.ds(pl.multiple_of(tp * quarter, quarter), quarter)]
     for n in range(3):
         frm = (tp + 3 - n) % 4
@@ -481,11 +490,17 @@
         part_w[i] = w.reshape(2, 4, 32, 256).astype(BF16)
         return carry
 
-    lax.fori_loop(0, 16, product, 0)
-    d = rcopy(part_w.at[:, other], mate_w, s_w.at[0, 0], r_w.at[0, 0], partner)
-    d.start()
-    sends.append(d)
-    d.wait_recv()
+    pieces = []
+    for n in range(4):
+        lax.fori_loop(4 * n, 4 * n + 4, product, 0)
+        d = rcopy(
+            part_w.at[4 * n : 4 * n + 4, other], mate_w.at[4 * n : 4 * n + 4], s_w.at[0, n], r_w.at[0, n], partner
+        )
+        d.start()
+        pieces.append(d)
+        sends.append(d)
+    for d in pieces:
+        d.wait_recv()
 
     def w_part(d, h):
         a = part_w[8 * h : 8 * h + 8, c, d]
@@ -496,34 +511,27 @@
     ring_x.near(w_part)
     ring_x.middle(w_part)
     first, second = ring_x.end(w_part)
-    acc_x[0:2] = first.reshape(2, 4, 32, 256)
-    acc_x[2:4] = second.reshape(2, 4, 32, 256)
-
-    def y_part(d, h):
-        return acc_x[2 * h : 2 * h + 2, d]
-
-    ring_y = Ring(y, yp, ym, (sy, ry), s_w.at[2], r_w.at[2])
-    ring_y.start(y_part)
-    ring_y.near(y_part)
-    ring_y.middle(y_part)
-    first, second = ring_y.end(y_part)
-    acc_y[0:2] = first
-    acc_y[2:4] = second
-
-    def z_part(d, h):
-        return acc_y[d, 16 * h : 16 * h + 16]
-
-    ring_z = Ring(z, zp, zm, (sz, rz), s_w.at[3], r_w.at[3])
-    ring_z.start(z_part)
-    ring_z.near(z_part)
-    ring_z.middle(z_part)
-    first, second = ring_z.end(z_part)
-    wg_ref[0:16] = first
-    wg_ref[16:32] = second
+    wsend[0:8] = first.astype(BF16)
+    wsend[8:16] = second.astype(BF16)
+    mine = zy(z, y)[0] // 2
+    for n, (dz, dy) in enumerate(offsets):
+        to = zy(z + dz, y + dy)
+        d = rcopy(wsend.at[to[0] // 2], wland.at[mine], s_d.at[n], r_d.at[n], to)
+        d.start()
+        sends.append(d)
+    acc_x[0:8] = first
+    acc_x[8:16] = second
+    total = acc_x[mine]
+    for n, (dz, dy) in enumerate(offsets):
+        frm = zy(z - dz, y - dy)
+        slot = wland.at[frm[0] // 2]
+        rcopy(slot, slot, s_d.at[n], r_d.at[n], frm).wait_recv()
+        total = total + wland[frm[0] // 2].astype(F32)
+    wg_ref[...] = total
 
     for d in sends:
         d.wait_send()
-    for r in rings_a + rings_b + [ring_x, ring_y, ring_z]:
+    for r in rings_a + rings_b + [ring_x]:
         r.drain()
 
 
@@ -532,8 +540,8 @@
     return pl.pallas_call(
         reduce_kernel,
         out_shape=[
-            jax.ShapeDtypeStruct((SEQS, ROWS, HD), BF16),
-            jax.ShapeDtypeStruct((SEQS, ROWS, HD), BF16),
+            jax.ShapeDtypeStruct((SEQS, HD, ROWS), BF16),
+            jax.ShapeDtypeStruct((SEQS, HD, ROWS), BF16),
             jax.ShapeDtypeStruct((32, 256), F32),
         ],
         in_specs=[pl.BlockSpec(memory_space=v)] * 2,
@@ -549,19 +557,20 @@
             v((192, 256), BF16),
             v((16, 2, 4, 32, 256), BF16),
             v((16, 4, 32, 256), BF16),
-            v((4, 4, 32, 256), F32),
-            v((4, 32, 256), F32),
+            v((16, 32, 256), F32),
+            v((16, 32, 256), BF16),
+            v((16, 32, 256), BF16),
             *[v((6, 8, 32, 256), BF16) for _ in range(2)],
-            *[v((6, 2, 32, 256), BF16) for _ in range(2)],
-            *[v((6, 16, 256), BF16) for _ in range(2)],
             pltpu.SemaphoreType.DMA((8,)),
             pltpu.SemaphoreType.DMA((8,)),
             pltpu.SemaphoreType.DMA((4, 6)),
             pltpu.SemaphoreType.DMA((4, 6)),
             pltpu.SemaphoreType.DMA((3,)),
             pltpu.SemaphoreType.DMA((3,)),
-            pltpu.SemaphoreType.DMA((4, 6)),
-            pltpu.SemaphoreType.DMA((4, 6)),
+            pltpu.SemaphoreType.DMA((2, 6)),
+            pltpu.SemaphoreType.DMA((2, 6)),
+            pltpu.SemaphoreType.DMA((15,)),
+            pltpu.SemaphoreType.DMA((15,)),
         ],
         compiler_params=pltpu.CompilerParams(
             collective_id=1, has_side_effects=True, vmem_limit_bytes=44 * 2**20
@@ -571,10 +580,13 @@
 
 
 def on_device(queries, key_states, value_states, cotangent, gate_logits, layer_input, chosen):
-    kv_all = gather_kv(key_states, value_states)
-    query_grad, table = attend(chosen.reshape(-1), kv_all, queries, cotangent, gate_logits)
+    def turned(a):
+        return jnp.swapaxes(a, 1, 2)
+
+    kv_all = gather_kv(turned(key_states), turned(value_states))
+    query_grad, table = attend(chosen, kv_all, queries, cotangent, turned(gate_logits))
     key_grad, value_grad, weight_grad = reduce_grads(table, layer_input)
-    return query_grad, key_grad, value_grad, weight_grad
+    return query_grad, turned(key_grad), turned(value_grad), weight_grad
 
 
 def solution(mesh):

time: 122 us -> 111 us (0.910)
  Pallas kernels: 111 us -> 106 us
  local copies, waits for them, and re-layouts: 7.89 us -> 3.77 us
    unnamed x14 -> x17, local copies, waits for them, and re-layouts: 7.81 us -> 3.77 us
    pallas_call x1, Pallas kernels: 57.4 us -> 53.4 us  [reduce_grads(): pl.pallas_call(reduce_kernel, out_shape=[jax.ShapeDtypeStruct((SEQS, HD,...]
    pallas_call x1, Pallas kernels: 24.2 us -> 22.5 us  [attend(): pl.pallas_call(attend_kernel, grid_spec=pltpu.PrefetchScalarGridSpec(num_...]
where the time goes in v1:
time: 111 us; the launch traced here: 110 us
  Pallas kernels  106 us (95%)
  local copies, waits for them, and re-layouts  3.77 us (3%)
    pallas_call x1, Pallas kernels, reduce_grads(): pl.pallas_call(reduce_kernel, out_shape=[jax.ShapeDtypeStruct((SEQS, HD,...  53.4 us
    pallas_call x1, Pallas kernels, gather_kv(): pl.pallas_call(gather_kernel, out_shape=jax.ShapeDtypeStruct((SEQS, DEVS,...  29.8 us
    pallas_call x1, Pallas kernels, attend(): pl.pallas_call(attend_kernel, grid_spec=pltpu.PrefetchScalarGridSpec(num_...  22.5 us
    unnamed x17, local copies, waits for them, and re-layouts  3.77 us

profile of v1, /device:TPU:0, one launch (start us, length us, event | category | flops | bytes accessed | tf_op | source)
XLA Modules:
  0.0 110.2 jit_solution(1463489837419010297)
XLA Ops:
  0.6 0.0 copy-start.2
  0.6 0.0 copy-start.1
  0.7 0.0 copy-start.3
  0.7 1.0 copy-done.3
  1.6 0.0 copy-start.4
  1.6 0.9 copy-done.4
  2.5 0.0 copy-start.5
  2.5 0.0 copy-start.6
  2.5 0.0 copy-start
  2.5 29.8 %gather_kv.1 = bf16[2,32,384,128]{3,2,1,0:T(8,128)(2,1)S(1)} custom-call(bf16[2,64,384]{2,1,0:T(8,128)(2,1)S(1)} %bitcast.11, bf16[2,64,384]{2,1,0:T(8,128)(2,1)S(1)} %bitcast.12), custom_call_target="tpu_custom_call" | custom-call | tf_op jit(solution)/shard_map/gather_kv/pallas_call | solution.py:175
  32.3 0.0 copy-done.2
  32.3 0.0 copy-done.1
  32.3 0.0 copy-done.5
  32.3 0.0 copy-done.6
  32.3 22.5 %attend.1 = (bf16[2,384,256]{2,1,0:T(8,128)(2,1)}, bf16[2,192,64,128]{3,2,1,0:T(8,128)(2,1)S(1)}) custom-call(s32[2,6,1,16]{3,2,1,0:T(1,128)S(1)} %copy-done.6, bf16[2,192,64,128]{3,2,1,0:T(8,128)(2,1)S(1)} %bitcast.7, bf16[2,384,256]{2,1,0:T(8,128)(2,1)S(1)} %copy-done.1, bf16[2,384,256]{2,1,0:T(8,128)(2,1)S(1)} %copy-done.2, f32[2,4,384]{2,1,0:T(4,128)S(1)} %bitcast.13), custom_call_target="tpu_custom_call" | custom-call | tf_op jit(solution)/shard_map/attend/pallas_call | solution.py:286
  54.9 0.0 copy-done
  54.9 53.4 %reduce_grads.1 = (bf16[2,64,384]{2,1,0:T(8,128)(2,1)S(1)}, bf16[2,64,384]{2,1,0:T(8,128)(2,1)S(1)}, f32[32,256]{1,0:T(8,128)S(1)}) custom-call(bf16[2,4,4,2,384,128]{5,4,3,2,1,0:T(8,128)(2,1)S(1)} %bitcast.8, bf16[2,96,4096]{2,1,0:T(8,128)(2,1)S(1)} %copy-done), custom_call_target="tpu_custom_call" | custom-call | tf_op jit(solution)/shard_map/reduce_grads/pallas_call | solution.py:540
  108.3 0.6 copy.14
  108.9 0.6 copy.15
  109.6 0.6 copy.16
Async XLA Ops:
  0.6 31.7 %copy-start.2 = (bf16[2,384,256]{2,1,0:T(8,128)(2,1)S(1)}, bf16[2,384,256]{2,1,0:T(8,128)(2,1)}, u32[]{:S(2)}) copy-start(bf16[2,384,256]{2,1,0:T(8,128)(2,1)} %g_ref.1) | copy-start | bytes 1179652
  0.6 31.7 %copy-start.1 = (bf16[2,384,256]{2,1,0:T(8,128)(2,1)S(1)}, bf16[2,384,256]{2,1,0:T(8,128)(2,1)}, u32[]{:S(2)}) copy-start(bf16[2,384,256]{2,1,0:T(8,128)(2,1)} %q_ref.1) | copy-start | bytes 1179652
  0.7 1.0 copy-start.3
  1.6 0.9 copy-start.4
  2.5 29.8 %copy-start.5 = (f32[2,384,4]{1,2,0:T(4,128)S(1)}, f32[2,384,4]{1,2,0:T(4,128)}, u32[]{:S(2)}) copy-start(f32[2,384,4]{1,2,0:T(4,128)} %param.11) | copy-start | bytes 36868
  2.5 29.8 %copy-start.6 = (s32[2,6,1,16]{3,2,1,0:T(1,128)S(1)}, s32[2,6,1,16]{3,2,1,0:T(1,128)}, u32[]{:S(2)}) copy-start(s32[2,6,1,16]{3,2,1,0:T(1,128)} %ids_ref.1) | copy-start | bytes 2308
  2.5 52.4 %copy-start = (bf16[2,96,4096]{2,1,0:T(8,128)(2,1)S(1)}, bf16[2,96,4096]{2,1,0:T(8,128)(2,1)}, u32[]{:S(2)}) copy-start(bf16[2,96,4096]{2,1,0:T(8,128)(2,1)} %x_in.1) | copy-start | bytes 4718596
